TPU v7x, 512 devices: a whole 4x4x16 slice. The times are simulated.
512 devices in a mesh: sp: 128 (over z, x, core), tp: 4 (over y).
Axes of the slice: x: 4, y: 4, z: 16, core: 2. Of those that a mesh axis runs over, the one named last changes fastest.
Arguments:
- tokens: bfloat16 [16384, 2048], P(('sp', 'tp')), may hold values from -6 to 6
- input_norm_gain: float32 [2048], replicated, may hold values from 0.1 to 1.9
- convolution_value_weight: bfloat16 [2048, 1024], P('sp', 'tp'), may hold values from -0.125 to 0.125
- convolution_gate_weight: bfloat16 [2048, 1024], P('sp', 'tp'), may hold values from -0.125 to 0.125
- depthwise_filter_taps: float32 [31, 1024], P(None, 'tp'), may hold values from -4 to 4
- channel_norm_gain: float32 [1024], P('tp'), may hold values from 0.1 to 1.9
- channel_norm_bias: float32 [1024], P('tp'), may hold values from -3 to 3
- query_projection_weight: bfloat16 [2048, 1024], P('sp', 'tp'), may hold values from -0.125 to 0.125
- forget_gate_weight: bfloat16 [2048, 1024], P('sp', 'tp'), may hold values from -0.125 to 0.125
- recurrence_value_weight: bfloat16 [2048, 1024], P('sp', 'tp'), may hold values from -0.125 to 0.125
- output_gate_weight: bfloat16 [2048, 1024], P('sp', 'tp'), may hold values from -0.125 to 0.125
- forget_floor_margin: float32 [1024], P('tp'), may hold values from 6.1035156e-06 to 0.1
- decay_jump_terms: float32 [8, 16384], P('tp', 'sp'), may hold values from -0.7 to 0
- head_norm_gain: float32 [1024], P('tp'), may hold values from 0.1 to 1.9
- convolution_output_weight: bfloat16 [1024, 2048], P('tp', 'sp'), may hold values from -0.125 to 0.125
- recurrence_output_weight: bfloat16 [1024, 2048], P('tp', 'sp'), may hold values from -0.125 to 0.125
Outputs:
- mixed: bfloat16 [16384, 2048], P(('sp', 'tp'))
All inputs are finite; a program needn't handle non-finite values.
Results may differ from a plain program's by a relative error of at most 0.015.
Values may be sent and summed in bfloat16 or wider, within the bound.
A program may use at most 64 MiB of HBM per device.

v0:
```python
import jax
import jax.numpy as jnp
from jax import lax
from jax.sharding import Mesh
from jax.sharding import PartitionSpec as P

CONV_CH = 1024
HG_DK = 128
HG_DV = 128
HG_BLOCK = 64
SP = ("sp_0", "sp_1", "sp_2")
SP_TP = ("sp_0", "sp_1", "sp_2", "tp")
norm_eps = 1e-06
layer_eps = 1e-05


def rows_first(arrays, axis, dims):
    turned = [jnp.moveaxis(a, dim, 0) for a, dim in zip(arrays, dims)]
    both = jnp.concatenate([t.reshape(len(t), -1) for t in turned], axis=1)
    out, at, outs = (lax.all_gather(both, axis, axis=0, tiled=True), 0, [])
    for t, dim in zip(turned, dims):
        section = out[:, at : at + t[0].size].reshape(-1, *t.shape[1:])
        outs.append(jnp.moveaxis(section, 0, dim))
        at += t[0].size
    return tuple(outs)


def joined_along(blocks, dim):
    shape = list(blocks.shape[1:])
    shape[dim] *= blocks.shape[0]
    return jnp.moveaxis(blocks, 0, dim).reshape(shape)


def sent_to_all(x, axis):
    copies = jnp.broadcast_to(x, (lax.axis_size(axis), *x.shape))
    return lax.all_to_all(copies, axis, split_axis=0, concat_axis=0, tiled=True)


def gather_directly(x, axis, dim):
    return joined_along(sent_to_all(x, axis), dim)


def passed_along(value, axis, steps):
    count = lax.axis_size(axis)
    initial, last = (max(0, -steps), min(count, count - steps))
    return lax.ppermute(value, axis, [(source, source + steps) for source in range(initial, last)])


def filled_with(x, identity):
    return jax.tree.map(
        lambda part, zero: jnp.zeros_like(part) + jnp.asarray(zero, part.dtype), x, identity
    )


def entering(x, axes, combine, identity):
    before = start = filled_with(x, identity)
    running = x
    for axis in reversed(axes):
        size, mine = (lax.axis_size(axis), lax.axis_index(axis))
        pieces = jax.tree.map(
            lambda part, kind: lax.all_gather(part.astype(kind), axis),
            running,
            (jnp.bfloat16, jnp.bfloat16),
        )
        inside, running = (start, start)
        for k in range(size):
            passed = k < mine
            running = combine(
                running, jax.tree.map(lambda part, own: part[k].astype(own.dtype), pieces, x)
            )
            inside = jax.tree.map(lambda new, old: jnp.where(passed, new, old), running, inside)
        before = combine(inside, before)
    return before


def of_everyone(x, axis):
    return sent_to_all(x, axis).sum(axis=0)


def together(arrays, axis):
    flat, at, outs = (jnp.concatenate([a.reshape(-1) for a in arrays]), 0, [])
    running = of_everyone(flat, axis)
    for a in arrays:
        outs.append(running[at : at + a.size].reshape(a.shape))
        at += a.size
    return tuple(outs)


def in_blocks(x, dim, size):
    shape = x.shape
    blocks = x.reshape(*shape[:dim], size, shape[dim] // size, *shape[dim + 1 :])
    return jnp.moveaxis(blocks, dim, 0)


def sent_and_summed(x, axis, dim):
    blocks = in_blocks(x, dim, lax.axis_size(axis))
    arrived = lax.all_to_all(blocks, axis, split_axis=0, concat_axis=0, tiled=True)
    return arrived.astype(jnp.float32).sum(axis=0)


def convolve(gated, kernel):
    return lax.conv_general_dilated(
        gated[None],
        kernel[:, None, :],
        (1,),
        "VALID",
        dimension_numbers=("NWC", "WIO", "NWC"),
        feature_group_count=gated.shape[1],
    )[0]


def channel_norm(values, first_sum, second_sum, gain, bias):
    mean_value = first_sum[:, None] / CONV_CH
    variance = second_sum[:, None] / CONV_CH - mean_value * mean_value
    shifted = (values - mean_value) * lax.rsqrt(variance + layer_eps) * gain + bias
    return jax.nn.silu(shifted).astype(jnp.bfloat16)


def gate_factors(query_projected, forget_projected, forget_floor_margin, decay_jump_rows):
    row_total_count = query_projected.shape[0]
    head_total_count = decay_jump_rows.shape[1]
    query_rows = jax.nn.silu(query_projected.astype(jnp.float32))
    log_forget_gate = jnp.logaddexp(
        jnp.log1p(-forget_floor_margin),
        jnp.log(forget_floor_margin) + jax.nn.log_sigmoid(forget_projected.astype(jnp.float32)),
    )
    key_gate_values = -jnp.expm1(log_forget_gate)
    log_decay_running = (
        log_forget_gate.reshape(row_total_count, head_total_count, -1) + decay_jump_rows[:, :, None]
    )
    return (
        query_rows.reshape(row_total_count, head_total_count, -1),
        key_gate_values.reshape(row_total_count, head_total_count, -1),
        log_decay_running,
    )


def finish(recurrent, gain, outgate_proj):
    row_total_count = recurrent.shape[0]
    scaled = recurrent * lax.rsqrt(
        jnp.mean(recurrent * recurrent, axis=2, keepdims=True) + norm_eps
    )
    gated_out = (
        scaled.reshape(row_total_count, -1) * gain * jax.nn.silu(outgate_proj.astype(jnp.float32))
    )
    return gated_out.astype(jnp.bfloat16)


def combine_states(first_part, second_part):
    return (
        first_part[0] + second_part[0],
        jnp.exp(second_part[0])[:, :, None] * first_part[1] + second_part[1],
    )


def carry_step(recurrence_state, block_parts):
    decay_end, contribution = block_parts
    return (jnp.exp(decay_end)[:, :, None] * recurrence_state + contribution, recurrence_state)


def per_device(
    tokens,
    input_norm_gain,
    convolution_value_weight,
    convolution_gate_weight,
    depthwise_filter_taps,
    channel_norm_gain,
    channel_norm_bias,
    query_projection_weight,
    forget_gate_weight,
    recurrence_value_weight,
    output_gate_weight,
    forget_floor_margin,
    decay_jump_terms,
    head_norm_gain,
    convolution_output_weight,
    recurrence_output_weight,
):
    features = tokens.astype(jnp.float32)
    normed = (
        features
        * lax.rsqrt(jnp.mean(features * features, axis=1, keepdims=True) + norm_eps)
        * input_norm_gain
    ).astype(jnp.bfloat16)
    gathered = rows_first(
        (
            convolution_value_weight,
            convolution_gate_weight,
            query_projection_weight,
            forget_gate_weight,
            recurrence_value_weight,
            output_gate_weight,
            convolution_output_weight,
            recurrence_output_weight,
        ),
        SP,
        (0, 0, 0, 0, 0, 0, 1, 1),
    )
    projection_weights = gathered[:6]
    conv_columns = gathered[6]
    rec_columns = gathered[7]

    def project(row_piece):
        return jnp.concatenate(
            [
                jnp.dot(row_piece, weight, preferred_element_type=jnp.float32).astype(jnp.bfloat16)
                for weight in projection_weights
            ],
            axis=1,
        )

    projected = project(gather_directly(normed, "tp", 0))
    offsets = []
    position = 0
    for weight in projection_weights[:-1]:
        position = position + weight.shape[1]
        offsets.append(position)
    value_proj, gate_proj, query_projected, forget_projected, input_proj, outgate_proj = jnp.split(
        projected, offsets, axis=1
    )
    row_total_count = value_proj.shape[0]
    rim_rows = depthwise_filter_taps.shape[0] - 1
    tail_value, tail_gate = passed_along(
        (value_proj[row_total_count - rim_rows :], gate_proj[row_total_count - rim_rows :]), SP, 1
    )
    value_ext = jnp.concatenate([tail_value, value_proj], axis=0)
    gate_ext = jnp.concatenate([tail_gate, gate_proj], axis=0)
    gated = value_ext.astype(jnp.float32) * jax.nn.sigmoid(gate_ext.astype(jnp.float32))
    convolved = convolve(gated, depthwise_filter_taps).astype(jnp.bfloat16)
    device_heads = decay_jump_terms.shape[0]
    query_rows, key_gate_values, log_decay_running = gate_factors(
        query_projected, forget_projected, forget_floor_margin, decay_jump_terms.T
    )
    input_rows = input_proj.astype(jnp.float32).reshape(row_total_count, device_heads, -1)
    block_count = row_total_count // HG_BLOCK

    def to_blocks(array):
        return array.reshape(block_count, HG_BLOCK, device_heads, -1).transpose(0, 2, 1, 3)

    block_queries = to_blocks(query_rows)
    block_keys = to_blocks(key_gate_values)
    block_inputs = to_blocks(input_rows)
    cumulative = jnp.cumsum(to_blocks(log_decay_running), axis=2)
    final_decay = cumulative[:, :, -1, :]
    query_rows_scaled = block_queries * jnp.exp(cumulative)
    scaled_keys = block_keys * jnp.exp(-cumulative)
    final_keys = block_keys * jnp.exp(final_decay[:, :, None, :] - cumulative)
    attention_scores = jnp.einsum("nhtk,nhsk->nhts", query_rows_scaled, scaled_keys)
    causal = jnp.arange(HG_BLOCK)[:, None] >= jnp.arange(HG_BLOCK)[None, :]
    attention_scores = jnp.where(causal[None, None], attention_scores, 0.0)
    inner = jnp.einsum("nhts,nhsv->nhtv", attention_scores, block_inputs)
    contributions = jnp.einsum("nhsk,nhsv->nhkv", final_keys, block_inputs)
    initial = jnp.zeros((device_heads, HG_DK, HG_DV), jnp.float32)
    local_state, block_starts = lax.scan(carry_step, initial, (final_decay, contributions))
    device_decay = jnp.sum(final_decay, axis=0)
    before_blocks = jnp.cumsum(final_decay, axis=0) - final_decay
    incoming = entering(
        (device_decay, local_state),
        SP,
        combine_states,
        (jnp.zeros_like(device_decay), jnp.zeros_like(local_state)),
    )
    starts = block_starts + jnp.exp(before_blocks)[:, :, :, None] * incoming[1][None]
    recurrent = inner + jnp.einsum("nhtk,nhkv->nhtv", query_rows_scaled, starts)
    recurrent = recurrent.transpose(0, 2, 1, 3).reshape(row_total_count, device_heads, -1)
    rec_out = finish(recurrent, head_norm_gain, outgate_proj)
    values = convolved.astype(jnp.float32)
    totals = together((jnp.sum(values, axis=1), jnp.sum(values * values, axis=1)), "tp")
    conv_out = channel_norm(values, totals[0], totals[1], channel_norm_gain, channel_norm_bias)
    conv_part = lax.slice_in_dim(
        conv_out, 0, row_total_count // lax.axis_size("tp") * lax.axis_size("tp"), axis=0
    )
    summed = sent_and_summed(
        (
            jnp.dot(conv_part, conv_columns, preferred_element_type=jnp.float32)
            + jnp.dot(rec_out, rec_columns, preferred_element_type=jnp.float32)
        ).astype(jnp.bfloat16),
        "tp",
        0,
    )
    return summed.astype(jnp.bfloat16)


def solution(mesh):
    split = Mesh(mesh.devices.reshape(16, 4, 2, mesh.shape["tp"]), ("sp_0", "sp_1", "sp_2", "tp"))
    return jax.shard_map(
        per_device,
        mesh=split,
        in_specs=(
            P(SP_TP, None),
            P(),
            P(SP, "tp"),
            P(SP, "tp"),
            P(None, "tp"),
            P("tp"),
            P("tp"),
            P(SP, "tp"),
            P(SP, "tp"),
            P(SP, "tp"),
            P(SP, "tp"),
            P("tp"),
            P("tp", SP),
            P("tp"),
            P("tp", SP),
            P("tp", SP),
        ),
        out_specs=P(SP_TP, None),
        check_vma=False,
    )
```

profile of v0, /device:TPU:6, one launch (start us, length us, event | category | flops | bytes accessed | tf_op | source)
XLA Modules:
  0.0 284.3 jit_solution(15545226052518464159)
XLA Ops:
  12.8 1.0 fusion.18
  15.8 4.5 %all-to-all-start = ((bf16[4,32,2048]{2,1,0:T(8,128)(2,1)}), bf16[4,32,2048]{2,1,0:T(8,128)(2,1)S(1)}, u32[]{:S(2)}, u32[]{:S(2)}) async-start(bf16[4,32,2048]{2,1,0:T(8,128)(2,1)} %broadcast_in_dim.27), calls=%async_computation | async-start | bytes 1048576 | tf_op jit(solution)/shard_map/all_to_all | solution.py:36
  21.7 8.0 %all-to-all-done = bf16[4,32,2048]{2,1,0:T(8,128)(2,1)S(1)} async-done(((bf16[4,32,2048]{2,1,0:T(8,128)(2,1)}), bf16[4,32,2048]{2,1,0:T(8,128)(2,1)S(1)}, u32[]{:S(2)}, u32[]{:S(2)}) %all-to-all-start) | async-done | bytes 524320 | tf_op jit(solution)/shard_map/all_to_all | solution.py:36
  29.7 132.8 %all-gather.6.cloned.1.call-done = bf16[2048,2048]{1,0:T(8,128)(2,1)} async-done(((bf16[16,2048]{1,0:T(8,128)(2,1)}), bf16[2048,2048]{1,0:T(8,128)(2,1)}) %all-gather.6.cloned.1.call-update) | async-done | bytes 8388624 | tf_op jit(solution)/shard_map/all_gather | solution.py:20
  162.5 1.7 exponential-minus-one_negate_fusion
  164.7 1.5 convolution_convert_fusion.2
  166.9 1.9 all-gather.1
  168.8 1.8 all-gather.2
  170.8 12.3 %all_gather.35 = bf16[4,2,128,128]{3,2,1,0:T(8,128)(2,1)S(1)} all-gather(bf16[1,2,128,128]{3,2,1,0:T(8,128)(2,1)S(1)} %fusion.63), channel_id=1, replica_groups=mesh['sp_0'=16,'sp_1'=4,'sp_2'=2,'tp'=4] {'sp_1'}, dimensions={0}, use_global_device_ids=true | all-gather | bytes 327680 | tf_op jit(solution)/shard_map/all_gather | solution.py:61
  183.0 8.5 %all_gather.31 = bf16[4,2,128]{2,1,0:T(2,128)(2,1)S(1)} all-gather(bf16[1,2,128]{2,1,0:T(2,128)(2,1)S(1)} %get-tuple-element.87), channel_id=1, replica_groups=mesh['sp_0'=16,'sp_1'=4,'sp_2'=2,'tp'=4] {'sp_1'}, dimensions={0}, use_global_device_ids=true | all-gather | bytes 2560 | tf_op jit(solution)/shard_map/all_gather | solution.py:61
  192.4 1.6 divide_multiply_fusion.1
  194.0 1.5 convolution_convert_fusion.6
  195.6 1.9 collective-permute-start
  197.5 1.5 convolution_convert_fusion.5
  199.1 4.9 %collective-permute-start.1 = (bf16[30,256]{1,0:T(8,128)(2,1)S(1)}, bf16[30,256]{1,0:T(8,128)(2,1)S(1)}, u32[]{:S(2)}, u32[]{:S(2)}) collective-permute-start(bf16[30,256]{1,0:T(8,128)(2,1)S(1)} %slice.237), channel_id=1, source_target_pairs={{0,4},{4,8},{8,12},{12,16},{16,20},{20,24},{24,28},{28,32},{32,36}... | collective-permute-start | bytes 46088 | tf_op jit(solution)/shard_map/ppermute | solution.py:46
  203.9 26.1 %all_gather.32 = bf16[16,2,128]{2,1,0:T(2,128)(2,1)S(1)} all-gather(bf16[1,2,128]{2,1,0:T(2,128)(2,1)S(1)} %get-tuple-element.83), channel_id=1, replica_groups=mesh['sp_0'=16,'sp_1'=4,'sp_2'=2,'tp'=4] {'sp_0'}, dimensions={0}, use_global_device_ids=true | all-gather | bytes 8704 | tf_op jit(solution)/shard_map/all_gather | solution.py:61
  230.4 2.2 fusion.97
  233.3 4.3 %all-to-all-start.1 = ((f32[4,1,256]{2,1,0:T(1,128)}), f32[4,1,256]{2,1,0:T(1,128)S(1)}, u32[]{:S(2)}, u32[]{:S(2)}) async-start(f32[4,1,256]{2,1,0:T(1,128)} %broadcast_in_dim.29), calls=%async_computation.1 | async-start | bytes 8192 | tf_op jit(solution)/shard_map/all_to_all | solution.py:36
  237.6 5.3 %all-to-all-done.1 = f32[4,1,256]{2,1,0:T(1,128)S(1)} async-done(((f32[4,1,256]{2,1,0:T(1,128)}), f32[4,1,256]{2,1,0:T(1,128)S(1)}, u32[]{:S(2)}, u32[]{:S(2)}) %all-to-all-start.1) | async-done | bytes 4128 | tf_op jit(solution)/shard_map/all_to_all | solution.py:36
  243.0 1.7 fusion.14
  244.7 14.4 %all-gather.8.cloned.1.call-done = bf16[16,2,128,128]{3,2,1,0:T(8,128)(2,1)} async-done(((bf16[1,2,128,128]{3,2,1,0:T(8,128)(2,1)}), bf16[16,2,128,128]{3,2,1,0:T(8,128)(2,1)}) %all-gather.8.cloned.1.call-update) | async-done | bytes 1048592 | tf_op jit(solution)/shard_map/all_gather | solution.py:61
  259.1 2.1 fusion.38
  262.1 2.5 fusion
  264.5 12.2 %all_to_all.16 = bf16[4,32,2048]{2,1,0:T(8,128)(2,1)S(1)} all-to-all(bf16[4,32,2048]{2,1,0:T(8,128)(2,1)S(1)} %bitcast.162), channel_id=1, replica_groups=mesh['sp_0'=16,'sp_1'=4,'sp_2'=2,'tp'=4] {'tp'}, dimensions={0} | all-to-all | bytes 1048576 | tf_op jit(solution)/shard_map/all_to_all | solution.py:97
  (71 shorter events, 14.7 us)
Async XLA Ops:
  6.5 223.9 %copy-start = (f32[31,256]{1,0:T(8,128)S(1)}, f32[31,256]{1,0:T(8,128)}, u32[]{:S(2)}) copy-start(f32[31,256]{1,0:T(8,128)} %param.22) | copy-start | bytes 95236
  6.5 156.0 %all-gather.6.cloned.1.call-start = ((), (), s32[]{:S(2)}) async-start(), calls=%async_computation.3 | async-start | bytes 8454144 | tf_op jit(solution)/shard_map/all_gather | solution.py:20
  12.1 0.6 copy-start.1
  15.8 13.9 %all-to-all-start = ((bf16[4,32,2048]{2,1,0:T(8,128)(2,1)}), bf16[4,32,2048]{2,1,0:T(8,128)(2,1)S(1)}, u32[]{:S(2)}, u32[]{:S(2)}) async-start(bf16[4,32,2048]{2,1,0:T(8,128)(2,1)} %broadcast_in_dim.27), calls=%async_computation | async-start | bytes 1048576 | tf_op jit(solution)/shard_map/all_to_all | solution.py:36
  20.2 238.9 %all-gather.8.cloned.1.call-start = ((), (), s32[]{:S(2)}) async-start(), calls=%async_computation.4 | async-start | bytes 1114112 | tf_op jit(solution)/shard_map/all_gather | solution.py:61
  166.2 76.7 %copy-start.2 = (f32[256]{0:T(256)S(1)}, f32[256]{0:T(256)}, u32[]{:S(2)}) copy-start(f32[256]{0:T(256)} %param.24) | copy-start | bytes 3076
  166.2 76.7 %copy-start.3 = (f32[256]{0:T(256)S(1)}, f32[256]{0:T(256)}, u32[]{:S(2)}) copy-start(f32[256]{0:T(256)} %param.23) | copy-start | bytes 3076
  170.8 91.3 %copy-start.4 = (f32[256]{0:T(256)S(1)}, f32[256]{0:T(256)}, u32[]{:S(2)}) copy-start(f32[256]{0:T(256)} %param.31) | copy-start | bytes 3076
  195.6 34.7 %collective-permute-start = (bf16[30,256]{1,0:T(8,128)(2,1)S(1)}, bf16[30,256]{1,0:T(8,128)(2,1)S(1)}, u32[]{:S(2)}, u32[]{:S(2)}) collective-permute-start(bf16[30,256]{1,0:T(8,128)(2,1)S(1)} %slice.235), channel_id=1, source_target_pairs={{0,4},{4,8},{8,12},{12,16},{16,20},{20,24},{24,28},{28,32},{32,36}... | collective-permute-start | bytes 46088 | tf_op jit(solution)/shard_map/ppermute | solution.py:46
  199.1 31.3 %collective-permute-start.1 = (bf16[30,256]{1,0:T(8,128)(2,1)S(1)}, bf16[30,256]{1,0:T(8,128)(2,1)S(1)}, u32[]{:S(2)}, u32[]{:S(2)}) collective-permute-start(bf16[30,256]{1,0:T(8,128)(2,1)S(1)} %slice.237), channel_id=1, source_target_pairs={{0,4},{4,8},{8,12},{12,16},{16,20},{20,24},{24,28},{28,32},{32,36}... | collective-permute-start | bytes 46088 | tf_op jit(solution)/shard_map/ppermute | solution.py:46
  233.3 9.6 %all-to-all-start.1 = ((f32[4,1,256]{2,1,0:T(1,128)}), f32[4,1,256]{2,1,0:T(1,128)S(1)}, u32[]{:S(2)}, u32[]{:S(2)}) async-start(f32[4,1,256]{2,1,0:T(1,128)} %broadcast_in_dim.29), calls=%async_computation.1 | async-start | bytes 8192 | tf_op jit(solution)/shard_map/all_to_all | solution.py:36
Sparse Core Ops, SparseCore 0:
  12.9 149.5 all-gather.5
  192.5 66.5 all-gather.7
where the time goes:
time: 285 us; the launch traced here: 284 us
  waiting for transfers between devices  161 us (56%)
  blocking collectives  62.7 us (22%)
  starting transfers between devices  15.5 us (5%)
  matrix products  15.2 us (5%)
  between operations  13.7 us (5%)
  local copies, waits for them, and re-layouts  9.17 us (3%)
  other arithmetic  7.39 us (3%)
    all_gather x1, waiting for transfers between devices, rows_first(): out, at, outs = (lax.all_gather(both, axis, axis=0, tiled=True), 0, [])  133 us
    all_gather x5, blocking collectives, entering(): lax.all_gather(part.astype(kind), axis)  50.5 us
    all_gather x1, waiting for transfers between devices, entering(): lax.all_gather(part.astype(kind), axis)  14.4 us
    all_to_all x2, waiting for transfers between devices, sent_to_all(): return lax.all_to_all(copies, axis, split_axis=0, concat_axis=0, tiled=True)  13.3 us
    all_to_all x1, blocking collectives, sent_and_summed(): lax.all_to_all(blocks, axis, split_axis=0, concat_axis=0, tiled=True)  12.2 us
    all_to_all x2, starting transfers between devices, sent_to_all(): return lax.all_to_all(copies, axis, split_axis=0, concat_axis=0, tiled=True)  8.75 us
    dot_general x5, matrix products, project(): jnp.dot(row_piece, weight, preferred_element_type=jnp.float32)  7.87 us
    ppermute x2, starting transfers between devices, passed_along(): lax.ppermute(value, axis, [(source, source + steps) for source in range(i...  6.78 us
  transfers between devices with their start and end apart: 6, of which 4 were waited for; matrix products, arithmetic and copies ran while one was open for 5% of the time, Pallas kernels for 0%

commit v1 on v0

--- a/solution.py
+++ b/solution.py
@@ -14,10 +14,17 @@
 layer_eps = 1e-05
 
 
+def all_by_exchange(x, mesh_axis, along):
+    devices = lax.axis_size(mesh_axis)
+    pieces = jnp.stack([x for _ in range(devices)])
+    pieces = lax.all_to_all(pieces, mesh_axis, split_axis=0, concat_axis=0)
+    return jnp.concatenate(pieces, axis=along)
+
+
 def rows_first(arrays, axis, dims):
     turned = [jnp.moveaxis(a, dim, 0) for a, dim in zip(arrays, dims)]
     both = jnp.concatenate([t.reshape(len(t), -1) for t in turned], axis=1)
-    out, at, outs = (lax.all_gather(both, axis, axis=0, tiled=True), 0, [])
+    out, at, outs = (all_by_exchange(both, axis, 0), 0, [])
     for t, dim in zip(turned, dims):
         section = out[:, at : at + t[0].size].reshape(-1, *t.shape[1:])
         outs.append(jnp.moveaxis(section, 0, dim))

time: 285 us -> 537 us (1.88)
  waiting for transfers between devices: 161 us -> 385 us
  starting transfers between devices: 15.5 us -> 34.1 us
  blocking collectives: 62.7 us -> 68.5 us
    all_to_all x0 -> x1, waiting for transfers between devices: none -> 363 us  [all_by_exchange(): pieces = lax.all_to_all(pieces, mesh_axis, split_axis=0, concat_axis=0)]
    all_gather x1 -> x0, waiting for transfers between devices: 133 us -> none  [rows_first(): out, at, outs = (lax.all_gather(both, axis, axis=0, tiled=True), 0, [])]
    all_to_all x0 -> x1, starting transfers between devices: none -> 20 us  [all_by_exchange(): pieces = lax.all_to_all(pieces, mesh_axis, split_axis=0, concat_axis=0)]
    all_gather x5, blocking collectives: 50.5 us -> 56.3 us  [entering(): lax.all_gather(part.astype(kind), axis)]
  transfers between devices with their start and end apart: 6 -> 6, of which waited for: 4 -> 4; matrix products, arithmetic and copies ran while one was open for 5% -> 2% of each run, Pallas kernels for 0% -> 0%
where the time goes in v1:
time: 537 us; the launch traced here: 536 us
  waiting for transfers between devices  385 us (72%)
  blocking collectives  68.5 us (13%)
  starting transfers between devices  34.1 us (6%)
  matrix products  15.2 us (3%)
  between operations  13.8 us (3%)
  local copies, waits for them, and re-layouts  12.1 us (2%)
  other arithmetic  6.71 us (1%)
    all_to_all x1, waiting for transfers between devices, all_by_exchange(): pieces = lax.all_to_all(pieces, mesh_axis, split_axis=0, concat_axis=0)  363 us
    all_gather x5, blocking collectives, entering(): lax.all_gather(part.astype(kind), axis)  56.3 us
    all_to_all x1, starting transfers between devices, all_by_exchange(): pieces = lax.all_to_all(pieces, mesh_axis, split_axis=0, concat_axis=0)  20 us
    all_gather x1, waiting for transfers between devices, entering(): lax.all_gather(part.astype(kind), axis)  12.7 us
    all_to_all x1, blocking collectives, sent_and_summed(): lax.all_to_all(blocks, axis, split_axis=0, concat_axis=0, tiled=True)  12.2 us
  transfers between devices with their start and end apart: 6, of which 4 were waited for; matrix products, arithmetic and copies ran while one was open for 2% of the time, Pallas kernels for 0%

profile of v1, /device:TPU:6, one launch (start us, length us, event | category | flops | bytes accessed | tf_op | source)
XLA Modules:
  0.0 535.6 jit_solution(11815351215714003366)
XLA Ops:
  9.4 4.5 all-to-all-start
  19.5 3.9 all-to-all-done
  23.4 4.3 stack.2
  27.7 20.0 %all-to-all-start.1 = ((bf16[128,16,2048]{2,1,0:T(8,128)(2,1)}), bf16[128,16,2048]{2,1,0:T(8,128)(2,1)}, u32[]{:S(2)}, u32[]{:S(2)}) async-start(bf16[128,16,2048]{2,1,0:T(8,128)(2,1)} %stack.2), calls=%async_computation.1 | async-start | bytes 16777216 | tf_op jit(solution)/shard_map/all_to_all | solution.py:20
  47.9 363.4 %all-to-all-done.1 = bf16[128,16,2048]{2,1,0:T(8,128)(2,1)} async-done(((bf16[128,16,2048]{2,1,0:T(8,128)(2,1)}), bf16[128,16,2048]{2,1,0:T(8,128)(2,1)}, u32[]{:S(2)}, u32[]{:S(2)}) %all-to-all-start.1) | async-done | bytes 8388640 | tf_op jit(solution)/shard_map/all_to_all | solution.py:20
  412.8 1.6 divide_multiply_fusion.1
  414.3 1.5 convolution_convert_fusion.6
  415.9 1.7 exponential-minus-one_negate_fusion
  418.7 1.9 all-gather.1
  420.6 1.8 all-gather.2
  422.6 14.2 %all_gather.31 = bf16[4,2,128,128]{3,2,1,0:T(8,128)(2,1)S(1)} all-gather(bf16[1,2,128,128]{3,2,1,0:T(8,128)(2,1)S(1)} %fusion.63), channel_id=1, replica_groups=mesh['sp_0'=16,'sp_1'=4,'sp_2'=2,'tp'=4] {'sp_1'}, dimensions={0}, use_global_device_ids=true | all-gather | bytes 327680 | tf_op jit(solution)/shard_map/all_gather | solution.py:68
  436.8 9.1 %all_gather.27 = bf16[4,2,128]{2,1,0:T(2,128)(2,1)S(1)} all-gather(bf16[1,2,128]{2,1,0:T(2,128)(2,1)S(1)} %get-tuple-element.87), channel_id=1, replica_groups=mesh['sp_0'=16,'sp_1'=4,'sp_2'=2,'tp'=4] {'sp_1'}, dimensions={0}, use_global_device_ids=true | all-gather | bytes 2560 | tf_op jit(solution)/shard_map/all_gather | solution.py:68
  446.9 1.9 collective-permute-start
  448.8 1.5 convolution_convert_fusion.5
  450.4 4.5 collective-permute-start.1
  454.9 29.3 %all_gather.28 = bf16[16,2,128]{2,1,0:T(2,128)(2,1)S(1)} all-gather(bf16[1,2,128]{2,1,0:T(2,128)(2,1)S(1)} %get-tuple-element.83), channel_id=1, replica_groups=mesh['sp_0'=16,'sp_1'=4,'sp_2'=2,'tp'=4] {'sp_0'}, dimensions={0}, use_global_device_ids=true | all-gather | bytes 8704 | tf_op jit(solution)/shard_map/all_gather | solution.py:68
  484.6 2.2 fusion.97
  487.5 3.2 all-to-all-start.2
  490.8 5.2 all-to-all-done.2
  496.1 1.7 fusion.14
  497.8 12.7 %all-gather.5.cloned.1.call-done = bf16[16,2,128,128]{3,2,1,0:T(8,128)(2,1)} async-done(((bf16[1,2,128,128]{3,2,1,0:T(8,128)(2,1)}), bf16[16,2,128,128]{3,2,1,0:T(8,128)(2,1)}) %all-gather.5.cloned.1.call-update) | async-done | bytes 1048592 | tf_op jit(solution)/shard_map/all_gather | solution.py:68
  510.5 2.1 fusion.38
  513.4 2.5 fusion
  515.9 12.2 %all_to_all.21 = bf16[4,32,2048]{2,1,0:T(8,128)(2,1)S(1)} all-to-all(bf16[4,32,2048]{2,1,0:T(8,128)(2,1)S(1)} %bitcast.163), channel_id=1, replica_groups=mesh['sp_0'=16,'sp_1'=4,'sp_2'=2,'tp'=4] {'tp'}, dimensions={0} | all-to-all | bytes 1048576 | tf_op jit(solution)/shard_map/all_to_all | solution.py:104
  (73 shorter events, 15.3 us)
Async XLA Ops:
  6.5 478.0 %copy-start = (f32[31,256]{1,0:T(8,128)S(1)}, f32[31,256]{1,0:T(8,128)}, u32[]{:S(2)}) copy-start(f32[31,256]{1,0:T(8,128)} %param.22) | copy-start | bytes 95236
  9.4 13.9 %all-to-all-start = ((bf16[4,32,2048]{2,1,0:T(8,128)(2,1)}), bf16[4,32,2048]{2,1,0:T(8,128)(2,1)S(1)}, u32[]{:S(2)}, u32[]{:S(2)}) async-start(bf16[4,32,2048]{2,1,0:T(8,128)(2,1)} %broadcast_in_dim.27), calls=%async_computation | async-start | bytes 1048576 | tf_op jit(solution)/shard_map/all_to_all | solution.py:43
  27.7 20.1 %copy-start.4 = (f32[2,128]{1,0:T(2,128)S(1)}, f32[2,128]{1,0:T(2,128)}, u32[]{:S(2)}) copy-start(f32[2,128]{1,0:T(2,128)} %param.30) | copy-start | bytes 3076
  27.7 20.2 %copy-start.5 = (f32[256]{0:T(256)S(1)}, f32[256]{0:T(256)}, u32[]{:S(2)}) copy-start(f32[256]{0:T(256)} %param.29) | copy-start | bytes 3076
  27.7 383.6 %all-to-all-start.1 = ((bf16[128,16,2048]{2,1,0:T(8,128)(2,1)}), bf16[128,16,2048]{2,1,0:T(8,128)(2,1)}, u32[]{:S(2)}, u32[]{:S(2)}) async-start(bf16[128,16,2048]{2,1,0:T(8,128)(2,1)} %stack.2), calls=%async_computation.1 | async-start | bytes 16777216 | tf_op jit(solution)/shard_map/all_to_all | solution.py:20
  47.6 462.8 %all-gather.5.cloned.1.call-start = ((), (), s32[]{:S(2)}) async-start(), calls=%async_computation.4 | async-start | bytes 1114112 | tf_op jit(solution)/shard_map/all_gather | solution.py:68
  414.3 81.7 %copy-start.1 = (f32[256]{0:T(256)S(1)}, f32[256]{0:T(256)}, u32[]{:S(2)}) copy-start(f32[256]{0:T(256)} %param.24) | copy-start | bytes 3076
  414.3 81.7 %copy-start.2 = (f32[256]{0:T(256)S(1)}, f32[256]{0:T(256)}, u32[]{:S(2)}) copy-start(f32[256]{0:T(256)} %param.23) | copy-start | bytes 3076
  418.3 95.0 %copy-start.3 = (f32[256]{0:T(256)S(1)}, f32[256]{0:T(256)}, u32[]{:S(2)}) copy-start(f32[256]{0:T(256)} %param.31) | copy-start | bytes 3076
  446.9 37.6 %collective-permute-start = (bf16[30,256]{1,0:T(8,128)(2,1)S(1)}, bf16[30,256]{1,0:T(8,128)(2,1)S(1)}, u32[]{:S(2)}, u32[]{:S(2)}) collective-permute-start(bf16[30,256]{1,0:T(8,128)(2,1)S(1)} %slice.235), channel_id=1, source_target_pairs={{0,4},{4,8},{8,12},{12,16},{16,20},{20,24},{24,28},{28,32},{32,36}... | collective-permute-start | bytes 46088 | tf_op jit(solution)/shard_map/ppermute | solution.py:53
  450.4 34.1 %collective-permute-start.1 = (bf16[30,256]{1,0:T(8,128)(2,1)S(1)}, bf16[30,256]{1,0:T(8,128)(2,1)S(1)}, u32[]{:S(2)}, u32[]{:S(2)}) collective-permute-start(bf16[30,256]{1,0:T(8,128)(2,1)S(1)} %slice.237), channel_id=1, source_target_pairs={{0,4},{4,8},{8,12},{12,16},{16,20},{20,24},{24,28},{28,32},{32,36}... | collective-permute-start | bytes 46088 | tf_op jit(solution)/shard_map/ppermute | solution.py:53
  487.5 8.5 %all-to-all-start.2 = ((f32[4,1,256]{2,1,0:T(1,128)}), f32[4,1,256]{2,1,0:T(1,128)S(1)}, u32[]{:S(2)}, u32[]{:S(2)}) async-start(f32[4,1,256]{2,1,0:T(1,128)} %broadcast_in_dim.29), calls=%async_computation.2 | async-start | bytes 8192 | tf_op jit(solution)/shard_map/all_to_all | solution.py:43
Sparse Core Ops, SparseCore 0:
  446.9 63.5 all-gather.4
